TPU v7x, 32 devices: a whole 2x2x4 slice. The times are simulated.
32 devices in a mesh: sp: 16 (over z, y, x), tp: 2 (over core).
Axes of the slice: x: 2, y: 2, z: 4, core: 2. Of those that a mesh axis runs over, the one named last changes fastest.
Arguments:
- tokens: bfloat16 [6144, 2048], P(('sp', 'tp')), may hold values from -6 to 6
- query_weight: bfloat16 [2048, 1024], P(None, 'tp'), may hold values from -0.125 to 0.125
- key_weight: bfloat16 [2048, 1024], P(None, 'tp'), may hold values from -0.125 to 0.125
- value_weight: bfloat16 [2048, 1024], P(None, 'tp'), may hold values from -0.125 to 0.125
- query_gain: float32 [64], replicated, may hold values from 0.5 to 16
- key_gain: float32 [64], replicated, may hold values from 0.5 to 16
- log_gate_total: float32 [6144, 16], P('sp', 'tp'), may hold values from -877 to 0, as said below
- output_weight: bfloat16 [1024, 2048], P('tp'), may hold values from -0.1875 to 0.1875
Outputs:
- mixed: bfloat16 [6144, 2048], P(('sp', 'tp'))
Inputs may be any that keep to these rules, and one draw needn't show every extreme that they name: `log_gate_total`: each column never rises from one position to the next.
All inputs are finite; a program needn't handle non-finite values.
Results may differ from a plain program's by a relative error of at most 0.014.
The roundings to bfloat16 on the way count: a program that leaves them out, or rounds other values in their place, can miss the bound.
Values may be sent and summed in bfloat16 or wider, within the bound.
A program may use at most 128 MiB of HBM per device.

v0:
```python
import math
import jax
import jax.numpy as jnp
from jax import lax
from jax.sharding import PartitionSpec as P

NORM_EPS = 1e-06


def head_norm(raw, gain, head_count):
    row_count = raw.shape[0]
    split = raw.reshape(row_count, head_count, -1)
    scaled = split * lax.rsqrt(jnp.mean(split * split, axis=-1, keepdims=True) + NORM_EPS) * gain
    return scaled.reshape(row_count, -1).astype(jnp.bfloat16)


def on_device(
    tokens,
    query_weight,
    key_weight,
    value_weight,
    query_gain,
    key_gain,
    log_gate_total,
    output_weight,
):
    attn_width = query_weight.shape[1]
    head_count = log_gate_total.shape[1]
    head_size = attn_width // head_count
    shard_rows = log_gate_total.shape[0]
    half_rows = shard_rows // 2
    sp_index = lax.axis_index("sp")
    score_scale = head_size ** (-0.5)
    pieces = lax.all_gather(tokens, "tp", axis=0, tiled=True)
    query_part = head_norm(
        jnp.dot(pieces, query_weight, preferred_element_type=jnp.float32), query_gain, head_count
    )
    key_part = head_norm(
        jnp.dot(pieces, key_weight, preferred_element_type=jnp.float32), key_gain, head_count
    )
    value_part = jnp.dot(pieces, value_weight, preferred_element_type=jnp.float32).astype(
        jnp.bfloat16
    )
    joined = jnp.stack([query_part, key_part, value_part], axis=0)
    queries = joined[0]
    key_value = joined[1:]
    gates_all = lax.all_gather(log_gate_total, "sp", axis=0, tiled=True)
    offsets = jnp.arange(shard_rows, dtype=jnp.int32)
    query_pos = sp_index * shard_rows + offsets
    query_heads = queries.reshape(shard_rows, head_count, head_size)
    gate_rows = log_gate_total.T
    halves = []
    for lower in (0, half_rows):
        pos_half = query_pos[lower : lower + half_rows]
        halves.append(
            (
                query_heads[lower : lower + half_rows],
                pos_half,
                gate_rows[:, lower : lower + half_rows],
                jnp.max(pos_half),
            )
        )
    half_state = (
        jnp.full((head_count, half_rows), -1e30, jnp.float32),
        jnp.zeros((head_count, half_rows), jnp.float32),
        jnp.zeros((head_count, half_rows, head_size), jnp.float32),
    )
    carry = (half_state, half_state)
    piece = lax.all_gather(key_value, "sp", axis=1, tiled=True)
    piece_rows = piece.shape[1]
    block_rows = math.gcd(piece_rows, 3072)
    block_count = piece_rows // block_rows
    key_blocks = piece[0].reshape(block_count, block_rows, head_count, head_size)
    value_blocks = piece[1].reshape(block_count, block_rows, head_count, head_size)
    gate_blocks = gates_all.reshape(block_count, block_rows, head_count)

    def one_block(state, inputs):
        key_block, value_block, key_gate, block_index = inputs
        block_start = block_index * block_rows
        key_pos = block_start + jnp.arange(block_rows, dtype=jnp.int32)
        key_gate_rows = key_gate.T
        updated = []
        for half_index in range(2):
            query_half, pos_half, gate_half, last_half = halves[half_index]

            def compute(current):
                running_max, running_sum, running_out = current
                scores = (
                    jnp.einsum(
                        "thd,shd->hts", query_half, key_block, preferred_element_type=jnp.float32
                    )
                    * score_scale
                )
                scores = scores + gate_half[:, :, None] - key_gate_rows[:, None, :]
                scores = jnp.where(
                    key_pos[None, None, :] <= pos_half[None, :, None], scores, -jnp.inf
                )
                new_max = jnp.maximum(running_max, jnp.max(scores, axis=2))
                rescale = jnp.exp(running_max - new_max)
                probs = jnp.exp(scores - new_max[:, :, None])
                running_sum = running_sum * rescale + jnp.sum(probs, axis=2)
                running_out = running_out * rescale[:, :, None] + jnp.einsum(
                    "hts,shd->htd",
                    probs.astype(jnp.bfloat16),
                    value_block,
                    preferred_element_type=jnp.float32,
                )
                return (new_max, running_sum, running_out)

            def keep_state(current):
                return current

            updated.append(
                lax.cond(block_start <= last_half, compute, keep_state, state[half_index])
            )
        return ((updated[0], updated[1]), None)

    carry, unused = lax.scan(
        one_block,
        carry,
        (key_blocks, value_blocks, gate_blocks, jnp.arange(block_count, dtype=jnp.int32)),
    )
    early_state, late_state = carry
    running_sum = jnp.concatenate([early_state[1], late_state[1]], axis=1)
    running_out = jnp.concatenate([early_state[2], late_state[2]], axis=1)
    attended = (
        (running_out / running_sum[:, :, None])
        .transpose(1, 0, 2)
        .reshape(shard_rows, attn_width)
        .astype(jnp.bfloat16)
    )
    mixed = lax.psum_scatter(
        jnp.dot(attended, output_weight, preferred_element_type=jnp.float32).astype(jnp.bfloat16),
        "tp",
        scatter_dimension=0,
        tiled=True,
    )
    return mixed


def solution(mesh):
    placed = (
        P(("sp", "tp"), None),
        P(None, "tp"),
        P(None, "tp"),
        P(None, "tp"),
        P(),
        P(),
        P("sp", "tp"),
        P("tp", None),
    )
    return jax.shard_map(
        on_device, mesh=mesh, in_specs=placed, out_specs=P(("sp", "tp"), None), check_vma=False
    )
```

profile of v0, /device:TPU:0, one launch (start us, length us, event | category | flops | bytes accessed | tf_op | source)
XLA Modules:
  0.0 426.1 jit_solution(7298764967293465248)
XLA Ops:
  8.0 13.4 %all-gather.3.cloned.1.call-done = bf16[384,2048]{1,0:T(8,128)(2,1)} async-done(((bf16[192,2048]{1,0:T(8,128)(2,1)}), bf16[384,2048]{1,0:T(8,128)(2,1)}) %all-gather.3.cloned.1.call-update) | async-done | bytes 1572880 | tf_op jit(solution)/shard_map/all_gather | solution.py:34
  21.4 4.2 fusion.28
  25.6 1.4 copy.13
  28.0 1.4 copy.14
  29.4 1.3 fusion.24
  30.8 3.0 fusion.22
  34.9 43.6 %all_gather.11 = f32[6144,8]{0,1:T(8,128)S(1)} all-gather(f32[384,8]{0,1:T(8,128)S(1)} %copy-done.7), channel_id=1, replica_groups=mesh['sp'=16,'tp'=2] {'sp'}, dimensions={0}, use_global_device_ids=true | all-gather | bytes 208896 | tf_op jit(solution)/shard_map/all_gather | solution.py:47
  79.4 4.2 fusion.29
  83.6 1.4 copy.17
  86.1 1.4 copy.18
  87.5 1.3 multiply_convert_fusion
  89.8 98.9 %all-gather.5.cloned.1.call-done = bf16[2,6144,512]{2,1,0:T(8,128)(2,1)} async-done(((bf16[2,384,512]{2,1,0:T(8,128)(2,1)}), bf16[2,6144,512]{2,1,0:T(8,128)(2,1)}) %all-gather.5.cloned.1.call-update) | async-done | bytes 12582928 | tf_op jit(solution)/shard_map/all_gather | solution.py:69
  188.7 10.1 %fusion.25 = (bf16[1,6144,512]{2,1,0:T(8,128)(2,1)}, bf16[1,6144,512]{2,1,0:T(8,128)(2,1)}) fusion(bf16[2,6144,512]{2,1,0:T(8,128)(2,1)} %all-gather.5.cloned.1.call-done), kind=kLoop, calls=%fused_computation.47 | loop fusion | bytes 25165824 | tf_op jit(solution)/shard_map/slice | solution.py:74
  198.8 16.2 %reshape.111 = bf16[2,3072,8,64]{3,2,1,0:T(8,128)(2,1)} reshape(bf16[1,6144,512]{2,1,0:T(8,128)(2,1)} %get-tuple-element.276) | data formatting | bytes 12582912 | tf_op jit(solution)/shard_map/reshape;squeeze | solution.py:73
  215.1 14.1 %copy.21 = bf16[2,3072,8,64]{1,3,2,0:T(8,128)(2,1)} copy(bf16[2,3072,8,64]{3,2,1,0:T(8,128)(2,1)} %reshape.111) | data formatting | bytes 12582912 | tf_op jit(solution)/shard_map/while | solution.py:118
  229.2 16.2 %reshape.112 = bf16[2,3072,8,64]{3,2,1,0:T(8,128)(2,1)} reshape(bf16[1,6144,512]{2,1,0:T(8,128)(2,1)} %get-tuple-element.275) | data formatting | bytes 12582912 | tf_op jit(solution)/shard_map/reshape;squeeze | solution.py:74
  245.4 14.0 %copy.22 = bf16[2,3072,8,64]{1,3,2,0:T(8,128)(2,1)} copy(bf16[2,3072,8,64]{3,2,1,0:T(8,128)(2,1)} %reshape.112) | data formatting | bytes 12582912 | tf_op jit(solution)/shard_map/while | solution.py:118
  260.4 83.1 %while.20 = (s32[]{:T(128)}, f32[8,192]{1,0:T(8,128)S(1)}, f32[8,192]{1,0:T(8,128)S(1)}, f32[8,192,64]{1,2,0:T(8,128)S(1)}, f32[8,192]{1,0:T(8,128)S(1)}, /*inde...) while((s32[]{:T(128)}, f32[8,192]{1,0:T(8,128)S(1)}, ...), condition=%wide.region_13.14_spmd, body=%wide.region_4.13_spmd.sunk | while | flops 2577933312 | bytes 325462240 | solution.py:118
  262.3 6.2 %dynamic-slice_bitcast_fusion.5 = (bf16[3072,8,64]{0,2,1:T(8,128)(2,1)}, bf16[3072,8,64]{0,2,1:T(8,128)(2,1)}) fusion(bf16[2,3072,8,64]{1,3,2,0:T(8,128)(2,1)} %get-tuple-element.483, s32[]{:T(128)S(6)} %copy.46, bf16[2,3072,8,64]{1,3,2,0:T(8,128)(2,1)} %get-tuple-element.481), kind=kLoop, calls=%fused_computation.26.clone.1 | loop fusion | bytes 12582916 | tf_op jit(solution)/shard_map/while/body/jit(dynamic_index_in_dim)/squeeze | solution.py:118
  268.5 32.1 %conditional.4 = ((f32[8,192]{1,0:T(8,128)S(1)}, f32[8,192]{1,0:T(8,128)S(1)}, f32[8,192,64]{1,2,0:T(8,128)S(1)})) conditional(s32[]{:T(128)} %convert_element_type.59, (f32[8,192]{1,0:T(8,128)S(1)}, f32[8,192]{1,0:T(8,128)S(1)}, f32[8,192,64]{1,2,0:T(8,128)S(1)}) %tuple.53, (s32[3072]{0:T(1024)S(1)}, s32[192]{0:T(256)S(1)}, ...), branch_computations={%region_5.5_spmd, %region_6.8_spmd} | conditional | flops 1288965120 | bytes 154762080 | solution.py:114
  268.9 7.2 %fusion.2 = (f32[8,192]{1,0:T(8,128)S(1)}, f32[8,192,3072]{2,1,0:T(8,128)S(1)}) fusion(f32[8,3072]{1,0:T(8,128)S(1)} %get-tuple-element.139, f32[8,192]{1,0:T(8,128)S(1)} %get-tuple-element.138, pred[192,3072]{1,0:T(8,128)(4,1)S(1)} %broadcast_compare_fusion, bf16[192,8,64]{0,2,1:T(8,128)(2,1)S(1)} %get-tuple-element.136, ...), kind=kOutput, calls=%fused_computation.4 | convolution fusion | flops 627571200 | bytes 22917120 | tf_op jit(solution)/shard_map/while/body/eval_jaxpr/cond/branch_1_fun/thd,shd->hts/dot_general | solution.py:89
  276.2 7.3 %copy-done.1 = f32[8,192,3072]{2,1,0:T(8,128)} copy-done((f32[8,192,3072]{2,1,0:T(8,128)}, f32[8,192,3072]{2,1,0:T(8,128)S(1)}, u32[]{:S(2)}) %copy-start.1) | copy-done | bytes 18874392 | tf_op jit(solution)/shard_map/while/body/eval_jaxpr/cond
  283.5 7.2 %fusion.1 = f32[8,192]{1,0:T(8,128)S(1)} fusion(f32[8,192,3072]{2,1,0:T(8,128)S(1)} %get-tuple-element.270, f32[8,192]{1,0:T(8,128)S(1)} %max.4, f32[8,3072]{1,0:T(8,128)S(1)} %get-tuple-element.139, f32[8,192]{1,0:T(8,128)S(1)} %get-tuple-element.138, pred[192,3072]{1,0:T(8,128)(4,1)S(1)} %broadcast_compare_fusion), kind=kLoop, calls=%fused_computation.3 | loop fusion | flops 28310016 | bytes 19580928 | tf_op jit(solution)/shard_map/while/body/eval_jaxpr/cond/branch_1_fun/reduce_sum | solution.py:101
  290.8 9.8 %fusion.6 = f32[8,192,64]{1,2,0:T(8,128)S(1)} fusion(bf16[3072,8,64]{0,2,1:T(8,128)(2,1)S(1)} %copy-done.3, f32[8,192,3072]{2,1,0:T(8,128)} %copy-done.1, f32[8,192]{1,0:T(8,128)S(1)} %max.4, f32[8,3072]{1,0:T(8,128)S(1)} %get-tuple-element.139, f32[8,192]{1,0:T(8,128)S(1)} %get-tuple-element.138, pred[192,3072]{1,0:T(8,128)(4,1)S(1)} %broadcast_compare_fusion, ...), kind=kOutput, calls=%fused_computation.7 | convolution fusion | flops 632487936 | bytes 23513088 | tf_op jit(solution)/shard_map/while/body/eval_jaxpr/cond/branch_1_fun/hts,shd->htd/dot_general | solution.py:102
  301.3 33.2 %conditional.5 = ((f32[8,192]{1,0:T(8,128)S(1)}, f32[8,192]{1,0:T(8,128)S(1)}, f32[8,192,64]{1,2,0:T(8,128)})) conditional(s32[]{:T(128)} %convert_element_type.60, (f32[8,192]{1,0:T(8,128)S(1)}, f32[8,192]{1,0:T(8,128)S(1)}, f32[8,192,64]{1,2,0:T(8,128)}) %tuple.55, (s32[3072]{0:T(1024)S(1)}, s32[192]{0:T(256)S(1)}, bf16[192,8,64]{0,2,1:T(8,128)(2,1)}, ...), branch_computations={%region_9.9_spmd, %region_10.12_spmd} | conditional | flops 1288965120 | bytes 157907872 | solution.py:114
  301.7 7.3 %fusion.13 = (f32[8,192]{1,0:T(8,128)S(1)}, f32[8,192,3072]{2,1,0:T(8,128)S(1)}) fusion(f32[8,3072]{1,0:T(8,128)S(1)} %get-tuple-element.149, f32[8,192]{1,0:T(8,128)S(1)} %get-tuple-element.148, pred[192,3072]{1,0:T(8,128)(4,1)S(1)} %broadcast_compare_fusion.1, bf16[192,8,64]{0,2,1:T(8,128)(2,1)} %get-tuple-element.146, ...), kind=kOutput, calls=%fused_computation.17 | convolution fusion | flops 627571200 | bytes 22917120 | tf_op jit(solution)/shard_map/while/body/eval_jaxpr/cond/branch_1_fun/thd,shd->hts/dot_general | solution.py:89
  309.1 7.5 %copy-done.2 = f32[8,192,3072]{2,1,0:T(8,128)} copy-done((f32[8,192,3072]{2,1,0:T(8,128)}, f32[8,192,3072]{2,1,0:T(8,128)S(1)}, u32[]{:S(2)}) %copy-start.2) | copy-done | bytes 18874392 | tf_op jit(solution)/shard_map/while/body/eval_jaxpr/cond
  316.6 7.2 %fusion.12 = f32[8,192]{1,0:T(8,128)S(1)} fusion(f32[8,192,3072]{2,1,0:T(8,128)S(1)} %get-tuple-element.272, f32[8,192]{1,0:T(8,128)S(1)} %max.5, f32[8,3072]{1,0:T(8,128)S(1)} %get-tuple-element.149, f32[8,192]{1,0:T(8,128)S(1)} %get-tuple-element.148, pred[192,3072]{1,0:T(8,128)(4,1)S(1)} %broadcast_compare_fusion.1), kind=kLoop, calls=%fused_computation.16 | loop fusion | flops 28310016 | bytes 19580928 | tf_op jit(solution)/shard_map/while/body/eval_jaxpr/cond/branch_1_fun/reduce_sum | solution.py:101
  323.9 9.8 %fusion.17 = f32[8,192,64]{1,2,0:T(8,128)S(1)} fusion(bf16[3072,8,64]{0,2,1:T(8,128)(2,1)S(1)} %copy-done.4, f32[8,192,3072]{2,1,0:T(8,128)} %copy-done.2, f32[8,192]{1,0:T(8,128)S(1)} %max.5, f32[8,3072]{1,0:T(8,128)S(1)} %get-tuple-element.149, f32[8,192]{1,0:T(8,128)S(1)} %get-tuple-element.148, pred[192,3072]{1,0:T(8,128)(4,1)S(1)} %broadcast_compare_fusion.1, ...), kind=kOutput, calls=%fused_computation.20 | convolution fusion | flops 632487936 | bytes 23513088 | tf_op jit(solution)/shard_map/while/body/eval_jaxpr/cond/branch_1_fun/hts,shd->htd/dot_general | solution.py:102
  336.5 6.2 %dynamic-slice_bitcast_fusion.5 = (bf16[3072,8,64]{0,2,1:T(8,128)(2,1)}, bf16[3072,8,64]{0,2,1:T(8,128)(2,1)}) fusion(bf16[2,3072,8,64]{1,3,2,0:T(8,128)(2,1)} %get-tuple-element.483, s32[]{:T(128)S(6)} %copy.46, bf16[2,3072,8,64]{1,3,2,0:T(8,128)(2,1)} %get-tuple-element.481), kind=kLoop, calls=%fused_computation.26.clone.1 | loop fusion | bytes 12582916 | tf_op jit(solution)/shard_map/while/body/jit(dynamic_index_in_dim)/squeeze | solution.py:118
  344.8 2.2 convolution_convert_fusion
  347.0 72.6 %reduce-scatter.2.cloned.1.call-done = bf16[192,2048]{1,0:T(8,128)(2,1)} async-done(((bf16[384,2048]{1,0:T(8,128)(2,1)}), bf16[192,2048]{1,0:T(8,128)(2,1)}) %reduce-scatter.2.cloned.1.call-update) | async-done | bytes 786448 | tf_op jit(solution)/shard_map/reduce_scatter | solution.py:132
  (64 shorter events, 11.7 us)
Async XLA Ops:
  6.5 338.2 %copy-start = (bf16[512,2048]{1,0:T(8,128)(2,1)S(1)}, bf16[512,2048]{1,0:T(8,128)(2,1)}, u32[]{:S(2)}) copy-start(bf16[512,2048]{1,0:T(8,128)(2,1)} %param.21) | copy-start | bytes 6291460
  6.5 28.3 %copy-start.8 = (f32[64]{0:T(128)S(1)}, f32[64]{0:T(128)}, u32[]{:S(2)}) copy-start(f32[64]{0:T(128)} %param.18) | copy-start | bytes 772
  6.5 28.4 %copy-start.7 = (f32[384,8]{0,1:T(8,128)S(1)}, f32[384,8]{0,1:T(8,128)}, u32[]{:S(2)}) copy-start(f32[384,8]{0,1:T(8,128)} %param.20) | copy-start | bytes 36868
  6.5 14.9 %all-gather.3.cloned.1.call-start = ((), (), s32[]{:S(2)}) async-start(), calls=%async_computation.1 | async-start | bytes 2359296 | tf_op jit(solution)/shard_map/all_gather | solution.py:34
  7.3 181.5 %all-gather.5.cloned.1.call-start = ((), (), s32[]{:S(2)}) async-start(), calls=%async_computation.2 | async-start | bytes 13369344 | tf_op jit(solution)/shard_map/all_gather | solution.py:69
  34.8 384.8 %reduce-scatter.2.cloned.1.call-start = ((), (), s32[]{:S(2)}) async-start(), calls=%async_computation.3 | async-start | bytes 2359296 | tf_op jit(solution)/shard_map/reduce_scatter | solution.py:132
  276.2 7.4 %copy-start.1 = (f32[8,192,3072]{2,1,0:T(8,128)}, f32[8,192,3072]{2,1,0:T(8,128)S(1)}, u32[]{:S(2)}) copy-start(f32[8,192,3072]{2,1,0:T(8,128)S(1)} %get-tuple-element.270) | copy-start | bytes 56623108 | tf_op jit(solution)/shard_map/while/body/eval_jaxpr/cond
  276.2 14.6 %copy-start.3 = (bf16[3072,8,64]{0,2,1:T(8,128)(2,1)S(1)}, bf16[3072,8,64]{0,2,1:T(8,128)(2,1)}, u32[]{:S(2)}) copy-start(bf16[3072,8,64]{0,2,1:T(8,128)(2,1)} %get-tuple-element.142) | copy-start | bytes 9437188 | tf_op jit(solution)/shard_map/while/body/eval_jaxpr/cond
  309.0 7.6 %copy-start.2 = (f32[8,192,3072]{2,1,0:T(8,128)}, f32[8,192,3072]{2,1,0:T(8,128)S(1)}, u32[]{:S(2)}) copy-start(f32[8,192,3072]{2,1,0:T(8,128)S(1)} %get-tuple-element.272) | copy-start | bytes 56623108 | tf_op jit(solution)/shard_map/while/body/eval_jaxpr/cond
  309.0 14.8 %copy-start.4 = (bf16[3072,8,64]{0,2,1:T(8,128)(2,1)S(1)}, bf16[3072,8,64]{0,2,1:T(8,128)(2,1)}, u32[]{:S(2)}) copy-start(bf16[3072,8,64]{0,2,1:T(8,128)(2,1)} %get-tuple-element.152) | copy-start | bytes 9437188 | tf_op jit(solution)/shard_map/while/body/eval_jaxpr/cond
  309.1 14.8 %copy-start.5 = (f32[8,192,64]{1,2,0:T(8,128)S(1)}, f32[8,192,64]{1,2,0:T(8,128)}, u32[]{:S(2)}) copy-start(f32[8,192,64]{1,2,0:T(8,128)} %get-tuple-element.151) | copy-start | bytes 1179652 | tf_op jit(solution)/shard_map/while/body/eval_jaxpr/cond
  333.7 0.8 copy-start.6
Sparse Core Ops, SparseCore 0:
  8.9 12.5 all-gather.2
  34.9 153.7 all-gather.4
  347.1 72.4 reduce-scatter.1
where the time goes:
time: 428 us; the launch traced here: 426 us
  waiting for transfers between devices  186 us (43%)
  local copies, waits for them, and re-layouts  110 us (26%)
  matrix products  47.8 us (11%)
  blocking collectives  43.6 us (10%)
  other arithmetic  21 us (5%)
  between operations  13.3 us (3%)
  loops' own time  4.31 us (1%)
    all_gather x1, waiting for transfers between devices, on_device(): piece = lax.all_gather(key_value, 'sp', axis=1, tiled=True)  98.9 us
    reduce_scatter x1, waiting for transfers between devices, on_device(): lax.psum_scatter(jnp.dot(attended, output_weight, preferred_element_type=...  72.6 us
    all_gather x1, blocking collectives, on_device(): gates_all = lax.all_gather(log_gate_total, 'sp', axis=0, tiled=True)  43.6 us
    while x2, local copies, waits for them, and re-layouts, on_device(): lax.scan(one_block, carry, (key_blocks, value_blocks, gate_blocks, jnp.ar...  28.2 us
    dot_general x2, matrix products, compute(): jnp.einsum('hts,shd->htd', probs.astype(jnp.bfloat16), value_block, prefe...  19.7 us
    another operation x1, local copies, waits for them, and re-layouts, on_device(): piece[0].reshape(block_count, block_rows, head_count, head_size)  16.2 us
    another operation x1, local copies, waits for them, and re-layouts, on_device(): piece[1].reshape(block_count, block_rows, head_count, head_size)  16.2 us
    cond x14, local copies, waits for them, and re-layouts  15.7 us
  transfers between devices with their start and end apart: 3, of which 3 were waited for; matrix products, arithmetic and copies ran while one was open for 3% of the time, Pallas kernels for 0%

commit v1 on v0

--- a/solution.py
+++ b/solution.py
@@ -66,7 +66,12 @@
         jnp.zeros((head_count, half_rows, head_size), jnp.float32),
     )
     carry = (half_state, half_state)
-    piece = lax.all_gather(key_value, "sp", axis=1, tiled=True)
+    ring = [key_value]
+    for hop in range(15):
+        ring.append(lax.ppermute(ring[-1], "sp", [(dev, (dev + 1) % 16) for dev in range(16)]))
+    piece = jnp.roll(
+        jnp.concatenate(ring[::-1], axis=1), (lax.axis_index("sp") + 1) * ring[0].shape[1], axis=1
+    )
     piece_rows = piece.shape[1]
     block_rows = math.gcd(piece_rows, 3072)
     block_count = piece_rows // block_rows

time: 428 us -> 655 us (1.53)
  waiting for transfers between devices: 186 us -> 343 us
  local copies, waits for them, and re-layouts: 110 us -> 172 us
    ppermute x0 -> x15, waiting for transfers between devices: none -> 259 us  [on_device(): lax.ppermute(ring[-1], 'sp', [(dev, (dev + 1) % 16) for dev in range(16)])]
    all_gather x1 -> x0, waiting for transfers between devices: 98.9 us -> none  [on_device(): piece = lax.all_gather(key_value, 'sp', axis=1, tiled=True)]
    unnamed x6 -> x82, local copies, waits for them, and re-layouts: 0.01 us -> 57 us
  transfers between devices with their start and end apart: 3 -> 17, of which waited for: 3 -> 16; matrix products, arithmetic and copies ran while one was open for 3% -> 2% of each run, Pallas kernels for 0% -> 0%
where the time goes in v1:
time: 655 us; the launch traced here: 653 us
  waiting for transfers between devices  343 us (52%)
  local copies, waits for them, and re-layouts  172 us (26%)
  matrix products  47.8 us (7%)
  blocking collectives  44.7 us (7%)
  other arithmetic  23.4 us (4%)
  between operations  13.6 us (2%)
    ppermute x15, waiting for transfers between devices, on_device(): lax.ppermute(ring[-1], 'sp', [(dev, (dev + 1) % 16) for dev in range(16)])  259 us
    reduce_scatter x1, waiting for transfers between devices, on_device(): lax.psum_scatter(jnp.dot(attended, output_weight, preferred_element_type=...  69.7 us
    unnamed x82, local copies, waits for them, and re-layouts  57 us
    all_gather x1, blocking collectives, on_device(): gates_all = lax.all_gather(log_gate_total, 'sp', axis=0, tiled=True)  44.7 us
    while x2, local copies, waits for them, and re-layouts, on_device(): lax.scan(one_block, carry, (key_blocks, value_blocks, gate_blocks, jnp.ar...  28.2 us
    dot_general x2, matrix products, compute(): jnp.einsum('hts,shd->htd', probs.astype(jnp.bfloat16), value_block, prefe...  19.7 us
    another operation x1, local copies, waits for them, and re-layouts, on_device(): piece[1].reshape(block_count, block_rows, head_count, head_size)  16.2 us
    another operation x1, local copies, waits for them, and re-layouts, on_device(): piece[0].reshape(block_count, block_rows, head_count, head_size)  16.2 us
  transfers between devices with their start and end apart: 17, of which 16 were waited for; matrix products, arithmetic and copies ran while one was open for 2% of the time, Pallas kernels for 0%

profile of v1, /device:TPU:0, one launch (start us, length us, event | category | flops | bytes accessed | tf_op | source)
XLA Modules:
  0.0 652.8 jit_solution(5658466188264515135)
XLA Ops:
  8.0 13.4 %all-gather.2.cloned.1.call-done = bf16[384,2048]{1,0:T(8,128)(2,1)} async-done(((bf16[192,2048]{1,0:T(8,128)(2,1)}), bf16[384,2048]{1,0:T(8,128)(2,1)}) %all-gather.2.cloned.1.call-update) | async-done | bytes 1572880 | tf_op jit(solution)/shard_map/all_gather | solution.py:34
  35.7 21.7 %collective-permute-done = bf16[2,384,512]{2,1,0:T(8,128)(2,1)S(1)} collective-permute-done((bf16[2,384,512]{2,1,0:T(8,128)(2,1)S(1)}, bf16[2,384,512]{2,1,0:T(8,128)(2,1)S(1)}, u32[]{:S(2)}, u32[]{:S(2)}) %collective-permute-start) | collective-permute-done | bytes 786464 | tf_op jit(solution)/shard_map/ppermute | solution.py:71
  58.3 22.5 %collective-permute-done.1 = bf16[2,384,512]{2,1,0:T(8,128)(2,1)S(1)} collective-permute-done((bf16[2,384,512]{2,1,0:T(8,128)(2,1)S(1)}, bf16[2,384,512]{2,1,0:T(8,128)(2,1)S(1)}, u32[]{:S(2)}, u32[]{:S(2)}) %collective-permute-start.1) | collective-permute-done | bytes 786464 | tf_op jit(solution)/shard_map/ppermute | solution.py:71
  81.7 21.7 %collective-permute-done.2 = bf16[2,384,512]{2,1,0:T(8,128)(2,1)S(1)} collective-permute-done((bf16[2,384,512]{2,1,0:T(8,128)(2,1)S(1)}, bf16[2,384,512]{2,1,0:T(8,128)(2,1)S(1)}, u32[]{:S(2)}, u32[]{:S(2)}) %collective-permute-start.2) | collective-permute-done | bytes 786464 | tf_op jit(solution)/shard_map/ppermute | solution.py:71
  104.3 20.8 %collective-permute-done.3 = bf16[2,384,512]{2,1,0:T(8,128)(2,1)S(1)} collective-permute-done((bf16[2,384,512]{2,1,0:T(8,128)(2,1)S(1)}, bf16[2,384,512]{2,1,0:T(8,128)(2,1)S(1)}, u32[]{:S(2)}, u32[]{:S(2)}) %collective-permute-start.3) | collective-permute-done | bytes 786464 | tf_op jit(solution)/shard_map/ppermute | solution.py:71
  126.0 20.0 %collective-permute-done.4 = bf16[2,384,512]{2,1,0:T(8,128)(2,1)S(1)} collective-permute-done((bf16[2,384,512]{2,1,0:T(8,128)(2,1)S(1)}, bf16[2,384,512]{2,1,0:T(8,128)(2,1)S(1)}, u32[]{:S(2)}, u32[]{:S(2)}) %collective-permute-start.4) | collective-permute-done | bytes 786464 | tf_op jit(solution)/shard_map/ppermute | solution.py:71
  146.9 19.1 %collective-permute-done.5 = bf16[2,384,512]{2,1,0:T(8,128)(2,1)S(1)} collective-permute-done((bf16[2,384,512]{2,1,0:T(8,128)(2,1)S(1)}, bf16[2,384,512]{2,1,0:T(8,128)(2,1)S(1)}, u32[]{:S(2)}, u32[]{:S(2)}) %collective-permute-start.5) | collective-permute-done | bytes 786464 | tf_op jit(solution)/shard_map/ppermute | solution.py:71
  166.9 18.3 %collective-permute-done.6 = bf16[2,384,512]{2,1,0:T(8,128)(2,1)S(1)} collective-permute-done((bf16[2,384,512]{2,1,0:T(8,128)(2,1)S(1)}, bf16[2,384,512]{2,1,0:T(8,128)(2,1)S(1)}, u32[]{:S(2)}, u32[]{:S(2)}) %collective-permute-start.6) | collective-permute-done | bytes 786464 | tf_op jit(solution)/shard_map/ppermute | solution.py:71
  186.1 17.4 %collective-permute-done.7 = bf16[2,384,512]{2,1,0:T(8,128)(2,1)S(1)} collective-permute-done((bf16[2,384,512]{2,1,0:T(8,128)(2,1)S(1)}, bf16[2,384,512]{2,1,0:T(8,128)(2,1)S(1)}, u32[]{:S(2)}, u32[]{:S(2)}) %collective-permute-start.7) | collective-permute-done | bytes 786464 | tf_op jit(solution)/shard_map/ppermute | solution.py:71
  204.4 16.7 %collective-permute-done.8 = bf16[2,384,512]{2,1,0:T(8,128)(2,1)S(1)} collective-permute-done((bf16[2,384,512]{2,1,0:T(8,128)(2,1)S(1)}, bf16[2,384,512]{2,1,0:T(8,128)(2,1)S(1)}, u32[]{:S(2)}, u32[]{:S(2)}) %collective-permute-start.8) | collective-permute-done | bytes 786464 | tf_op jit(solution)/shard_map/ppermute | solution.py:71
  222.1 16.8 %collective-permute-done.9 = bf16[2,384,512]{2,1,0:T(8,128)(2,1)S(1)} collective-permute-done((bf16[2,384,512]{2,1,0:T(8,128)(2,1)S(1)}, bf16[2,384,512]{2,1,0:T(8,128)(2,1)S(1)}, u32[]{:S(2)}, u32[]{:S(2)}) %collective-permute-start.9) | collective-permute-done | bytes 786464 | tf_op jit(solution)/shard_map/ppermute | solution.py:71
  239.8 17.8 %collective-permute-done.10 = bf16[2,384,512]{2,1,0:T(8,128)(2,1)S(1)} collective-permute-done((bf16[2,384,512]{2,1,0:T(8,128)(2,1)S(1)}, bf16[2,384,512]{2,1,0:T(8,128)(2,1)S(1)}, u32[]{:S(2)}, u32[]{:S(2)}) %collective-permute-start.10) | collective-permute-done | bytes 786464 | tf_op jit(solution)/shard_map/ppermute | solution.py:71
  258.5 19.7 %collective-permute-done.11 = bf16[2,384,512]{2,1,0:T(8,128)(2,1)} collective-permute-done((bf16[2,384,512]{2,1,0:T(8,128)(2,1)S(1)}, bf16[2,384,512]{2,1,0:T(8,128)(2,1)}, u32[]{:S(2)}, u32[]{:S(2)}) %collective-permute-start.11) | collective-permute-done | bytes 786464 | tf_op jit(solution)/shard_map/ppermute | solution.py:71
  278.3 44.7 %all_gather.7 = f32[6144,8]{0,1:T(8,128)S(1)} all-gather(f32[384,8]{0,1:T(8,128)S(1)} %copy-done.30), channel_id=1, replica_groups=mesh['sp'=16,'tp'=2] {'sp'}, dimensions={0}, use_global_device_ids=true | all-gather | bytes 208896 | tf_op jit(solution)/shard_map/all_gather | solution.py:47
  332.8 18.2 %collective-permute-done.13 = bf16[2,384,512]{2,1,0:T(8,128)(2,1)} collective-permute-done((bf16[2,384,512]{2,1,0:T(8,128)(2,1)}, bf16[2,384,512]{2,1,0:T(8,128)(2,1)}, u32[]{:S(2)}, u32[]{:S(2)}) %collective-permute-start.13) | collective-permute-done | bytes 786464 | tf_op jit(solution)/shard_map/ppermute | solution.py:71
  358.8 8.1 %collective-permute-done.14 = bf16[2,384,512]{2,1,0:T(8,128)(2,1)} collective-permute-done((bf16[2,384,512]{2,1,0:T(8,128)(2,1)}, bf16[2,384,512]{2,1,0:T(8,128)(2,1)}, u32[]{:S(2)}, u32[]{:S(2)}) %collective-permute-start.14) | collective-permute-done | bytes 786464 | tf_op jit(solution)/shard_map/ppermute | solution.py:71
  415.9 12.1 %constant_dynamic-slice_fusion.1 = (bf16[1,6144,512]{2,1,0:T(8,128)(2,1)}, bf16[1,6144,512]{2,1,0:T(8,128)(2,1)}) fusion(bf16[2,12288,512]{2,1,0:T(8,128)(2,1)} %constant_dynamic-update-slice_fusion, s32[]{:T(128)S(6)} %add.81, s32[]{:T(128)S(6)} %select_n.21), kind=kLoop, calls=%fused_computation.78 | loop fusion | bytes 25165832 | tf_op jit(solution)/shard_map/slice | solution.py:79
  428.1 16.2 %reshape.111 = bf16[2,3072,8,64]{3,2,1,0:T(8,128)(2,1)} reshape(bf16[1,6144,512]{2,1,0:T(8,128)(2,1)} %get-tuple-element.276) | data formatting | bytes 12582912 | tf_op jit(solution)/shard_map/reshape;squeeze | solution.py:78
  444.3 14.1 %copy.21 = bf16[2,3072,8,64]{1,3,2,0:T(8,128)(2,1)} copy(bf16[2,3072,8,64]{3,2,1,0:T(8,128)(2,1)} %reshape.111) | data formatting | bytes 12582912 | tf_op jit(solution)/shard_map/while | solution.py:123
  458.4 16.2 %reshape.112 = bf16[2,3072,8,64]{3,2,1,0:T(8,128)(2,1)} reshape(bf16[1,6144,512]{2,1,0:T(8,128)(2,1)} %get-tuple-element.275) | data formatting | bytes 12582912 | tf_op jit(solution)/shard_map/reshape;squeeze | solution.py:79
  474.6 14.1 %copy.22 = bf16[2,3072,8,64]{1,3,2,0:T(8,128)(2,1)} copy(bf16[2,3072,8,64]{3,2,1,0:T(8,128)(2,1)} %reshape.112) | data formatting | bytes 12582912 | tf_op jit(solution)/shard_map/while | solution.py:123
  489.6 83.1 %while.20 = (s32[]{:T(128)}, f32[8,192]{1,0:T(8,128)S(1)}, f32[8,192]{1,0:T(8,128)S(1)}, f32[8,192,64]{1,2,0:T(8,128)S(1)}, f32[8,192]{1,0:T(8,128)S(1)}, /*inde...) while((s32[]{:T(128)}, f32[8,192]{1,0:T(8,128)S(1)}, ...), condition=%wide.region_13.14_spmd, body=%wide.region_4.13_spmd.sunk | while | flops 2577933312 | bytes 325462176 | solution.py:123
  498.0 33.2 %conditional.5 = ((f32[8,192]{1,0:T(8,128)S(1)}, f32[8,192]{1,0:T(8,128)S(1)}, f32[8,192,64]{1,2,0:T(8,128)})) conditional(s32[]{:T(128)} %convert_element_type.60, (f32[8,192]{1,0:T(8,128)S(1)}, f32[8,192]{1,0:T(8,128)S(1)}, f32[8,192,64]{1,2,0:T(8,128)}) %tuple.55, (s32[3072]{0:T(1024)S(1)}, s32[192]{0:T(256)S(1)}, bf16[192,8,64]{0,2,1:T(8,128)(2,1)}, ...), branch_computations={%region_9.9_spmd, %region_10.12_spmd} | conditional | flops 1288965120 | bytes 157907872 | solution.py:119
  498.4 7.3 %fusion.13 = (f32[8,192]{1,0:T(8,128)S(1)}, f32[8,192,3072]{2,1,0:T(8,128)S(1)}) fusion(f32[8,3072]{1,0:T(8,128)S(1)} %get-tuple-element.149, f32[8,192]{1,0:T(8,128)S(1)} %get-tuple-element.148, pred[192,3072]{1,0:T(8,128)(4,1)S(1)} %broadcast_compare_fusion.1, bf16[192,8,64]{0,2,1:T(8,128)(2,1)} %get-tuple-element.146, ...), kind=kOutput, calls=%fused_computation.17 | convolution fusion | flops 627571200 | bytes 22917120 | tf_op jit(solution)/shard_map/while/body/eval_jaxpr/cond/branch_1_fun/thd,shd->hts/dot_general | solution.py:94
  505.8 7.5 %copy-done.1 = f32[8,192,3072]{2,1,0:T(8,128)} copy-done((f32[8,192,3072]{2,1,0:T(8,128)}, f32[8,192,3072]{2,1,0:T(8,128)S(1)}, u32[]{:S(2)}) %copy-start.1) | copy-done | bytes 18874392 | tf_op jit(solution)/shard_map/while/body/eval_jaxpr/cond
  520.5 9.8 %fusion.17 = f32[8,192,64]{1,2,0:T(8,128)S(1)} fusion(bf16[3072,8,64]{0,2,1:T(8,128)(2,1)S(1)} %copy-done.3, f32[8,192,3072]{2,1,0:T(8,128)} %copy-done.1, f32[8,192]{1,0:T(8,128)S(1)} %max.5, f32[8,3072]{1,0:T(8,128)S(1)} %get-tuple-element.149, f32[8,192]{1,0:T(8,128)S(1)} %get-tuple-element.148, pred[192,3072]{1,0:T(8,128)(4,1)S(1)} %broadcast_compare_fusion.1, ...), kind=kOutput, calls=%fused_computation.20 | convolution fusion | flops 632487936 | bytes 23513088 | tf_op jit(solution)/shard_map/while/body/eval_jaxpr/cond/branch_1_fun/hts,shd->htd/dot_general | solution.py:107
  531.8 32.1 %conditional.4 = ((f32[8,192]{1,0:T(8,128)S(1)}, f32[8,192]{1,0:T(8,128)S(1)}, f32[8,192,64]{1,2,0:T(8,128)S(1)})) conditional(s32[]{:T(128)} %convert_element_type.59, (f32[8,192]{1,0:T(8,128)S(1)}, f32[8,192]{1,0:T(8,128)S(1)}, f32[8,192,64]{1,2,0:T(8,128)S(1)}) %tuple.53, (s32[3072]{0:T(1024)S(1)}, s32[192]{0:T(256)S(1)}, ...), branch_computations={%region_5.5_spmd, %region_6.8_spmd} | conditional | flops 1288965120 | bytes 154762080 | solution.py:119
  532.2 7.2 %fusion.2 = (f32[8,192]{1,0:T(8,128)S(1)}, f32[8,192,3072]{2,1,0:T(8,128)S(1)}) fusion(f32[8,3072]{1,0:T(8,128)S(1)} %get-tuple-element.139, f32[8,192]{1,0:T(8,128)S(1)} %get-tuple-element.138, pred[192,3072]{1,0:T(8,128)(4,1)S(1)} %broadcast_compare_fusion, bf16[192,8,64]{0,2,1:T(8,128)(2,1)S(1)} %get-tuple-element.136, ...), kind=kOutput, calls=%fused_computation.4 | convolution fusion | flops 627571200 | bytes 22917120 | tf_op jit(solution)/shard_map/while/body/eval_jaxpr/cond/branch_1_fun/thd,shd->hts/dot_general | solution.py:94
  539.4 7.3 %copy-done.2 = f32[8,192,3072]{2,1,0:T(8,128)} copy-done((f32[8,192,3072]{2,1,0:T(8,128)}, f32[8,192,3072]{2,1,0:T(8,128)S(1)}, u32[]{:S(2)}) %copy-start.2) | copy-done | bytes 18874392 | tf_op jit(solution)/shard_map/while/body/eval_jaxpr/cond
  546.7 7.2 %fusion.1 = f32[8,192]{1,0:T(8,128)S(1)} fusion(f32[8,192,3072]{2,1,0:T(8,128)S(1)} %get-tuple-element.270, f32[8,192]{1,0:T(8,128)S(1)} %max.4, f32[8,3072]{1,0:T(8,128)S(1)} %get-tuple-element.139, f32[8,192]{1,0:T(8,128)S(1)} %get-tuple-element.138, pred[192,3072]{1,0:T(8,128)(4,1)S(1)} %broadcast_compare_fusion), kind=kLoop, calls=%fused_computation.3 | loop fusion | flops 28310016 | bytes 19580928 | tf_op jit(solution)/shard_map/while/body/eval_jaxpr/cond/branch_1_fun/reduce_sum | solution.py:106
  554.0 9.8 %fusion.6 = f32[8,192,64]{1,2,0:T(8,128)S(1)} fusion(bf16[3072,8,64]{0,2,1:T(8,128)(2,1)S(1)} %copy-done.4, f32[8,192,3072]{2,1,0:T(8,128)} %copy-done.2, f32[8,192]{1,0:T(8,128)S(1)} %max.4, f32[8,3072]{1,0:T(8,128)S(1)} %get-tuple-element.139, f32[8,192]{1,0:T(8,128)S(1)} %get-tuple-element.138, pred[192,3072]{1,0:T(8,128)(4,1)S(1)} %broadcast_compare_fusion, ...), kind=kOutput, calls=%fused_computation.7 | convolution fusion | flops 632487936 | bytes 23513088 | tf_op jit(solution)/shard_map/while/body/eval_jaxpr/cond/branch_1_fun/hts,shd->htd/dot_general | solution.py:107
  576.2 69.7 %reduce-scatter.2.cloned.1.call-done = bf16[192,2048]{1,0:T(8,128)(2,1)} async-done(((bf16[384,2048]{1,0:T(8,128)(2,1)}), bf16[192,2048]{1,0:T(8,128)(2,1)}) %reduce-scatter.2.cloned.1.call-update) | async-done | bytes 786448 | tf_op jit(solution)/shard_map/reduce_scatter | solution.py:137
  (169 shorter events, 119.1 us)
Async XLA Ops:
  6.5 567.5 %copy-start = (bf16[512,2048]{1,0:T(8,128)(2,1)S(1)}, bf16[512,2048]{1,0:T(8,128)(2,1)}, u32[]{:S(2)}) copy-start(bf16[512,2048]{1,0:T(8,128)(2,1)} %param.21) | copy-start | bytes 6291460
  6.5 271.7 %copy-start.31 = (f32[64]{0:T(128)S(1)}, f32[64]{0:T(128)}, u32[]{:S(2)}) copy-start(f32[64]{0:T(128)} %param.18) | copy-start | bytes 772
  6.5 271.8 %copy-start.30 = (f32[384,8]{0,1:T(8,128)S(1)}, f32[384,8]{0,1:T(8,128)}, u32[]{:S(2)}) copy-start(f32[384,8]{0,1:T(8,128)} %param.20) | copy-start | bytes 36868
  6.5 14.9 %all-gather.2.cloned.1.call-start = ((), (), s32[]{:S(2)}) async-start(), calls=%async_computation.1 | async-start | bytes 2359296 | tf_op jit(solution)/shard_map/all_gather | solution.py:34
  7.3 638.7 %reduce-scatter.2.cloned.1.call-start = ((), (), s32[]{:S(2)}) async-start(), calls=%async_computation.2 | async-start | bytes 2359296 | tf_op jit(solution)/shard_map/reduce_scatter | solution.py:137
  33.9 23.5 %collective-permute-start = (bf16[2,384,512]{2,1,0:T(8,128)(2,1)S(1)}, bf16[2,384,512]{2,1,0:T(8,128)(2,1)S(1)}, u32[]{:S(2)}, u32[]{:S(2)}) collective-permute-start(bf16[2,384,512]{2,1,0:T(8,128)(2,1)S(1)} %pad_maximum_fusion), channel_id=1, source_target_pairs={{0,2},{2,4},{4,6},{6,8},{8,10},{10,12},{12,14},{14,16},{16,18},{18... | collective-permute-start | bytes 2359304 | tf_op jit(solution)/shard_map/ppermute | solution.py:71
  58.2 22.5 %collective-permute-start.1 = (bf16[2,384,512]{2,1,0:T(8,128)(2,1)S(1)}, bf16[2,384,512]{2,1,0:T(8,128)(2,1)S(1)}, u32[]{:S(2)}, u32[]{:S(2)}) collective-permute-start(bf16[2,384,512]{2,1,0:T(8,128)(2,1)S(1)} %collective-permute-done), channel_id=1, source_target_pairs={{0,2},{2,4},{4,6},{6,8},{8,10},{10,12},{12,14},{14,16},{16,18},{18... | collective-permute-start | bytes 2359304 | tf_op jit(solution)/shard_map/ppermute | solution.py:71
  81.7 21.7 %collective-permute-start.2 = (bf16[2,384,512]{2,1,0:T(8,128)(2,1)S(1)}, bf16[2,384,512]{2,1,0:T(8,128)(2,1)S(1)}, u32[]{:S(2)}, u32[]{:S(2)}) collective-permute-start(bf16[2,384,512]{2,1,0:T(8,128)(2,1)S(1)} %collective-permute-done.1), channel_id=1, source_target_pairs={{0,2},{2,4},{4,6},{6,8},{8,10},{10,12},{12,14},{14,16},{16,18},{18... | collective-permute-start | bytes 2359304 | tf_op jit(solution)/shard_map/ppermute | solution.py:71
  104.3 20.8 %collective-permute-start.3 = (bf16[2,384,512]{2,1,0:T(8,128)(2,1)S(1)}, bf16[2,384,512]{2,1,0:T(8,128)(2,1)S(1)}, u32[]{:S(2)}, u32[]{:S(2)}) collective-permute-start(bf16[2,384,512]{2,1,0:T(8,128)(2,1)S(1)} %collective-permute-done.2), channel_id=1, source_target_pairs={{0,2},{2,4},{4,6},{6,8},{8,10},{10,12},{12,14},{14,16},{16,18},{18... | collective-permute-start | bytes 2359304 | tf_op jit(solution)/shard_map/ppermute | solution.py:71
  126.0 20.0 %collective-permute-start.4 = (bf16[2,384,512]{2,1,0:T(8,128)(2,1)S(1)}, bf16[2,384,512]{2,1,0:T(8,128)(2,1)S(1)}, u32[]{:S(2)}, u32[]{:S(2)}) collective-permute-start(bf16[2,384,512]{2,1,0:T(8,128)(2,1)S(1)} %collective-permute-done.3), channel_id=1, source_target_pairs={{0,2},{2,4},{4,6},{6,8},{8,10},{10,12},{12,14},{14,16},{16,18},{18... | collective-permute-start | bytes 2359304 | tf_op jit(solution)/shard_map/ppermute | solution.py:71
  146.9 19.1 %collective-permute-start.5 = (bf16[2,384,512]{2,1,0:T(8,128)(2,1)S(1)}, bf16[2,384,512]{2,1,0:T(8,128)(2,1)S(1)}, u32[]{:S(2)}, u32[]{:S(2)}) collective-permute-start(bf16[2,384,512]{2,1,0:T(8,128)(2,1)S(1)} %collective-permute-done.4), channel_id=1, source_target_pairs={{0,2},{2,4},{4,6},{6,8},{8,10},{10,12},{12,14},{14,16},{16,18},{18... | collective-permute-start | bytes 2359304 | tf_op jit(solution)/shard_map/ppermute | solution.py:71
  166.9 18.3 %collective-permute-start.6 = (bf16[2,384,512]{2,1,0:T(8,128)(2,1)S(1)}, bf16[2,384,512]{2,1,0:T(8,128)(2,1)S(1)}, u32[]{:S(2)}, u32[]{:S(2)}) collective-permute-start(bf16[2,384,512]{2,1,0:T(8,128)(2,1)S(1)} %collective-permute-done.5), channel_id=1, source_target_pairs={{0,2},{2,4},{4,6},{6,8},{8,10},{10,12},{12,14},{14,16},{16,18},{18... | collective-permute-start | bytes 2359304 | tf_op jit(solution)/shard_map/ppermute | solution.py:71
  186.1 17.4 %collective-permute-start.7 = (bf16[2,384,512]{2,1,0:T(8,128)(2,1)S(1)}, bf16[2,384,512]{2,1,0:T(8,128)(2,1)S(1)}, u32[]{:S(2)}, u32[]{:S(2)}) collective-permute-start(bf16[2,384,512]{2,1,0:T(8,128)(2,1)S(1)} %collective-permute-done.6), channel_id=1, source_target_pairs={{0,2},{2,4},{4,6},{6,8},{8,10},{10,12},{12,14},{14,16},{16,18},{18... | collective-permute-start | bytes 2359304 | tf_op jit(solution)/shard_map/ppermute | solution.py:71
  204.4 16.7 %collective-permute-start.8 = (bf16[2,384,512]{2,1,0:T(8,128)(2,1)S(1)}, bf16[2,384,512]{2,1,0:T(8,128)(2,1)S(1)}, u32[]{:S(2)}, u32[]{:S(2)}) collective-permute-start(bf16[2,384,512]{2,1,0:T(8,128)(2,1)S(1)} %collective-permute-done.7), channel_id=1, source_target_pairs={{0,2},{2,4},{4,6},{6,8},{8,10},{10,12},{12,14},{14,16},{16,18},{18... | collective-permute-start | bytes 2359304 | tf_op jit(solution)/shard_map/ppermute | solution.py:71
  222.1 16.8 %collective-permute-start.9 = (bf16[2,384,512]{2,1,0:T(8,128)(2,1)S(1)}, bf16[2,384,512]{2,1,0:T(8,128)(2,1)S(1)}, u32[]{:S(2)}, u32[]{:S(2)}) collective-permute-start(bf16[2,384,512]{2,1,0:T(8,128)(2,1)S(1)} %collective-permute-done.8), channel_id=1, source_target_pairs={{0,2},{2,4},{4,6},{6,8},{8,10},{10,12},{12,14},{14,16},{16,18},{18... | collective-permute-start | bytes 2359304 | tf_op jit(solution)/shard_map/ppermute | solution.py:71
  239.8 17.9 %collective-permute-start.10 = (bf16[2,384,512]{2,1,0:T(8,128)(2,1)S(1)}, bf16[2,384,512]{2,1,0:T(8,128)(2,1)S(1)}, u32[]{:S(2)}, u32[]{:S(2)}) collective-permute-start(bf16[2,384,512]{2,1,0:T(8,128)(2,1)S(1)} %collective-permute-done.9), channel_id=1, source_target_pairs={{0,2},{2,4},{4,6},{6,8},{8,10},{10,12},{12,14},{14,16},{16,18},{18... | collective-permute-start | bytes 2359304 | tf_op jit(solution)/shard_map/ppermute | solution.py:71
  258.5 19.7 %collective-permute-start.11 = (bf16[2,384,512]{2,1,0:T(8,128)(2,1)S(1)}, bf16[2,384,512]{2,1,0:T(8,128)(2,1)}, u32[]{:S(2)}, u32[]{:S(2)}) collective-permute-start(bf16[2,384,512]{2,1,0:T(8,128)(2,1)S(1)} %collective-permute-done.10), channel_id=1, source_target_pairs={{0,2},{2,4},{4,6},{6,8},{8,10},{10,12},{12,14},{14,16},{16,18},{18... | collective-permute-start | bytes 2359304 | tf_op jit(solution)/shard_map/ppermute | solution.py:71
  278.2 44.8 %collective-permute-start.12 = (bf16[2,384,512]{2,1,0:T(8,128)(2,1)}, bf16[2,384,512]{2,1,0:T(8,128)(2,1)}, u32[]{:S(2)}, u32[]{:S(2)}) collective-permute-start(bf16[2,384,512]{2,1,0:T(8,128)(2,1)} %collective-permute-done.11), channel_id=1, source_target_pairs={{0,2},{2,4},{4,6},{6,8},{8,10},{10,12},{12,14},{14,16},{16,18},{18... | collective-permute-start | bytes 2359304 | tf_op jit(solution)/shard_map/ppermute | solution.py:71
  323.0 28.0 %collective-permute-start.13 = (bf16[2,384,512]{2,1,0:T(8,128)(2,1)}, bf16[2,384,512]{2,1,0:T(8,128)(2,1)}, u32[]{:S(2)}, u32[]{:S(2)}) collective-permute-start(bf16[2,384,512]{2,1,0:T(8,128)(2,1)} %collective-permute-done.12), channel_id=1, source_target_pairs={{0,2},{2,4},{4,6},{6,8},{8,10},{10,12},{12,14},{14,16},{16,18},{18... | collective-permute-start | bytes 2359304 | tf_op jit(solution)/shard_map/ppermute | solution.py:71
  351.0 15.9 %collective-permute-start.14 = (bf16[2,384,512]{2,1,0:T(8,128)(2,1)}, bf16[2,384,512]{2,1,0:T(8,128)(2,1)}, u32[]{:S(2)}, u32[]{:S(2)}) collective-permute-start(bf16[2,384,512]{2,1,0:T(8,128)(2,1)} %collective-permute-done.13), channel_id=1, source_target_pairs={{0,2},{2,4},{4,6},{6,8},{8,10},{10,12},{12,14},{14,16},{16,18},{18... | collective-permute-start | bytes 2359304 | tf_op jit(solution)/shard_map/ppermute | solution.py:71
  358.8 33.5 %copy-start.10 = (bf16[2,384,512]{2,1,0:T(8,128)(2,1)S(1)}, bf16[2,384,512]{2,1,0:T(8,128)(2,1)}, u32[]{:S(2)}) copy-start(bf16[2,384,512]{2,1,0:T(8,128)(2,1)} %copy-done.9) | copy-start | bytes 2359300
  358.8 34.5 %copy-start.8 = (bf16[2,384,512]{2,1,0:T(8,128)(2,1)S(1)}, bf16[2,384,512]{2,1,0:T(8,128)(2,1)}, u32[]{:S(2)}) copy-start(bf16[2,384,512]{2,1,0:T(8,128)(2,1)} %copy-done.7) | copy-start | bytes 2359300
  358.8 35.4 %copy-start.6 = (bf16[2,384,512]{2,1,0:T(8,128)(2,1)S(1)}, bf16[2,384,512]{2,1,0:T(8,128)(2,1)}, u32[]{:S(2)}) copy-start(bf16[2,384,512]{2,1,0:T(8,128)(2,1)} %copy-done.5) | copy-start | bytes 2359300
  358.8 45.6 %copy-start.26 = (bf16[2,384,512]{2,1,0:T(8,128)(2,1)S(1)}, bf16[2,384,512]{2,1,0:T(8,128)(2,1)}, u32[]{:S(2)}) copy-start(bf16[2,384,512]{2,1,0:T(8,128)(2,1)} %copy-done.25) | copy-start | bytes 2359300
  358.8 46.5 %copy-start.24 = (bf16[2,384,512]{2,1,0:T(8,128)(2,1)S(1)}, bf16[2,384,512]{2,1,0:T(8,128)(2,1)}, u32[]{:S(2)}) copy-start(bf16[2,384,512]{2,1,0:T(8,128)(2,1)} %copy-done.23) | copy-start | bytes 2359300
  358.8 47.6 %copy-start.22 = (bf16[2,384,512]{2,1,0:T(8,128)(2,1)S(1)}, bf16[2,384,512]{2,1,0:T(8,128)(2,1)}, u32[]{:S(2)}) copy-start(bf16[2,384,512]{2,1,0:T(8,128)(2,1)} %copy-done.21) | copy-start | bytes 2359300
  358.8 48.5 %copy-start.20 = (bf16[2,384,512]{2,1,0:T(8,128)(2,1)S(1)}, bf16[2,384,512]{2,1,0:T(8,128)(2,1)}, u32[]{:S(2)}) copy-start(bf16[2,384,512]{2,1,0:T(8,128)(2,1)} %copy-done.19) | copy-start | bytes 2359300
  358.8 49.5 %copy-start.18 = (bf16[2,384,512]{2,1,0:T(8,128)(2,1)S(1)}, bf16[2,384,512]{2,1,0:T(8,128)(2,1)}, u32[]{:S(2)}) copy-start(bf16[2,384,512]{2,1,0:T(8,128)(2,1)} %copy-done.17) | copy-start | bytes 2359300
  369.0 40.2 %copy-start.16 = (bf16[2,384,512]{2,1,0:T(8,128)(2,1)S(1)}, bf16[2,384,512]{2,1,0:T(8,128)(2,1)}, u32[]{:S(2)}) copy-start(bf16[2,384,512]{2,1,0:T(8,128)(2,1)} %copy-done.15) | copy-start | bytes 2359300
  371.2 39.0 %copy-start.14 = (bf16[2,384,512]{2,1,0:T(8,128)(2,1)S(1)}, bf16[2,384,512]{2,1,0:T(8,128)(2,1)}, u32[]{:S(2)}) copy-start(bf16[2,384,512]{2,1,0:T(8,128)(2,1)} %copy-done.13) | copy-start | bytes 2359300
  373.4 37.8 %copy-start.12 = (bf16[2,384,512]{2,1,0:T(8,128)(2,1)S(1)}, bf16[2,384,512]{2,1,0:T(8,128)(2,1)}, u32[]{:S(2)}) copy-start(bf16[2,384,512]{2,1,0:T(8,128)(2,1)} %copy-done.11) | copy-start | bytes 2359300
  458.4 31.2 %copy-start.29 = (bf16[192,512]{0,1:T(8,128)(2,1)S(1)}, bf16[192,512]{0,1:T(8,128)(2,1)}, u32[]{:S(2)}) copy-start(bf16[192,512]{0,1:T(8,128)(2,1)} %copy.19) | copy-start | bytes 589828
  (17 other events, 69.8 us)
Sparse Core Ops, SparseCore 0:
  8.9 12.5 all-gather.1
  576.4 69.5 reduce-scatter.1
